TPU v7x, 768 devices: a whole 4x8x12 slice. The times are simulated.
768 devices in a mesh: ep: 24 (over z, core), tp: 32 (over y, x).
Axes of the slice: x: 4, y: 8, z: 12, core: 2. Of those that a mesh axis runs over, the one named last changes fastest.
Arguments:
- tokens: bfloat16 [3072, 2048], P('ep'), may hold values from -6 to 6
- norm_gain: float32 [2048], replicated, may hold values from 0.1 to 1.9
- route_ids: int32 [3072, 2], P('ep'), may hold values from 0 to 23, all different within a row; in each aligned block of 128 rows (0 to 127, 128 to 255, ...) at most 16 rows name the same one
- route_weights: float32 [3072, 2], P('ep'), may hold values from 0.05 to 1
- gate_proj: bfloat16 [24, 2048, 12288], P('ep', None, 'tp'), may hold values from -0.125 to 0.125
- up_proj: bfloat16 [24, 2048, 12288], P('ep', None, 'tp'), may hold values from -0.125 to 0.125
- down_proj: bfloat16 [24, 12288, 2048], P('ep', 'tp'), may hold values from -0.0546875 to 0.0546875
Outputs:
- mixed: bfloat16 [3072, 2048], P('ep', 'tp')
Inputs may be any that keep to these rules, and one draw needn't show every extreme that they name: `route_ids`: each token names 2 different experts; within the rows of one device (aligned blocks of 128 tokens) no expert is named by more than 16 pairs, a bound that some block reaches.
All inputs are finite; a program needn't handle non-finite values.
Results may differ from a plain program's by a relative error of at most 0.017.
Values may be sent and summed in bfloat16 or wider, within the bound.
A program may use at most 32 MiB of HBM per device.

v0:
```python
import jax
import jax.numpy as jnp
from jax import lax
from jax.sharding import PartitionSpec as P


def cut_along(array, dim, devices):
    before, after = (array.shape[:dim], array.shape[dim + 1 :])
    return jnp.moveaxis(array.reshape(*before, devices, -1, *after), dim, 0)


def sent_and_summed(array, axis, dim):
    devices = lax.axis_size(axis)
    blocks = lax.all_to_all(cut_along(array, dim, devices), axis, 0, 0, tiled=True)
    return jnp.sum(blocks.astype(jnp.float32), axis=0)


def local(tokens, norm_gain, route_ids, route_weights, gate_proj, up_proj, down_proj):
    ep_count = lax.axis_size("ep")
    tp_count = lax.axis_size("tp")
    tok_rows, width = tokens.shape
    topk = route_ids.shape[1]
    capacity = min(tok_rows, (3 * tok_rows * topk + 2 * ep_count - 1) // (2 * ep_count))
    share_width = width // tp_count
    values = tokens.astype(jnp.float32)
    mean_square = jnp.mean(values * values, axis=-1, keepdims=True)
    normed = (values * lax.rsqrt(mean_square + 1e-06) * norm_gain).astype(jnp.bfloat16)
    route_flat = route_ids.reshape(-1)
    onehot = (route_flat[:, None] == jnp.arange(ep_count, dtype=jnp.int32)[None, :]).astype(
        jnp.int32
    )
    slot_index = jnp.sum((jnp.cumsum(onehot, axis=0) - onehot) * onehot, axis=1)
    repeated = jnp.repeat(normed, topk, axis=0)
    down_local = down_proj[0]
    outgoing = (
        jnp.zeros((ep_count, capacity, width), jnp.bfloat16)
        .at[route_flat, slot_index]
        .set(repeated)
    )
    arrived = lax.all_to_all(outgoing, "ep", split_axis=0, concat_axis=0, tiled=True)
    item_rows = arrived.shape[1]
    merged_rows = arrived.reshape(-1, width)
    gate_act = jnp.dot(merged_rows, gate_proj[0], preferred_element_type=jnp.float32)
    up_act = jnp.dot(merged_rows, up_proj[0], preferred_element_type=jnp.float32)
    hidden = (jax.nn.silu(gate_act) * up_act).astype(jnp.bfloat16)
    term = lax.dot_general(
        down_local, hidden, (((0,), (1,)), ((), ())), preferred_element_type=jnp.float32
    )
    term = lax.optimization_barrier(term.astype(jnp.bfloat16))
    summed = sent_and_summed(term.astype(jnp.float32).astype(jnp.bfloat16), "tp", 0)
    back = summed.T.reshape(ep_count, item_rows, share_width)
    returned = lax.all_to_all(
        back.astype(jnp.bfloat16), "ep", split_axis=0, concat_axis=0, tiled=True
    ).astype(back.dtype)
    columns_back = returned.shape[2]
    picked = returned[route_flat, slot_index].reshape(tok_rows, topk, columns_back)
    weighted = jnp.sum(route_weights[:, :, None] * picked, axis=1)
    return weighted.astype(jnp.bfloat16)


def solution(mesh):
    placed = (
        P("ep", None),
        P(),
        P("ep", None),
        P("ep", None),
        P("ep", None, "tp"),
        P("ep", None, "tp"),
        P("ep", "tp", None),
    )
    return jax.shard_map(
        local, mesh=mesh, in_specs=placed, out_specs=P("ep", "tp"), check_vma=False
    )
```

profile of v0, /device:TPU:1, one launch (start us, length us, event | category | flops | bytes accessed | tf_op | source)
XLA Modules:
  0.0 191.5 jit_solution(11478509402015667183)
XLA Ops:
  0.0 0.0 copy-start
  0.0 0.9 copy.24
  0.9 0.1 eq.29
  1.0 0.1 eq.25
  1.2 0.1 reshape.85
  1.3 0.6 reduce-window.6
  1.9 0.2 slice_reduce_fusion
  2.2 1.2 fusion.12
  3.4 1.2 fusion.14
  4.7 0.6 broadcast_in_dim.5
  5.3 1.2 reshape.99
  6.5 0.1 fusion.25
  6.6 0.2 broadcast_in_dim.4
  6.8 33.3 %scatter_fusion = bf16[24,16,2048]{2,1,0:T(8,128)(2,1)S(1)} fusion(bf16[24,16,2048]{2,1,0:T(8,128)(2,1)S(1)} %broadcast_in_dim.4, s32[256]{0:T(256)S(1)} %bitcast.46, bf16[256,2048]{1,0:T(8,128)(2,1)} %reshape.99), kind=kCustom, calls=%fused_computation.1 | custom fusion | bytes 3147776 | tf_op jit(solution)/shard_map/scatter | solution.py:38
  40.1 0.0 copy-start.3
  40.1 72.7 %all_to_all.15 = bf16[24,16,2048]{2,1,0:T(8,128)(2,1)S(1)} all-to-all(bf16[24,16,2048]{2,1,0:T(8,128)(2,1)S(1)} %scatter_fusion), channel_id=1, replica_groups=mesh['ep'=24,'tp'=32] {'ep'}, dimensions={0} | all-to-all | bytes 3145728 | tf_op jit(solution)/shard_map/all_to_all | solution.py:40
  112.8 0.0 copy-start.1
  112.8 1.2 copy-done.1
  114.0 0.0 copy-done.3
  114.0 1.8 fusion.4
  115.8 0.0 copy-done
  115.8 3.8 %fusion = bf16[2048,384]{0,1:T(8,128)(2,1)S(1)} fusion(bf16[1,384,2048]{2,1,0:T(8,128)(2,1)S(1)} %copy-done, bf16[384,2048]{1,0:T(8,128)(2,1)} %bitcast.50, bf16[1,2048,384]{2,1,0:T(8,128)(2,1)} %param.12, f32[384,384]{1,0:T(8,128)} %fusion.4), kind=kOutput, calls=%fused_computation.3 | convolution fusion | flops 1209630720 | bytes 6881280 | tf_op jit(solution)/shard_map/dot_general | solution.py:46
  119.6 1.6 copy.28
  121.2 46.4 %all_to_all.16 = bf16[32,64,384]{2,1,0:T(8,128)(2,1)S(1)} all-to-all(bf16[32,64,384]{2,1,0:T(8,128)(2,1)} %bitcast.48), channel_id=1, replica_groups=mesh['ep'=24,'tp'=32] {'tp'}, dimensions={0} | all-to-all | bytes 3145728 | tf_op jit(solution)/shard_map/all_to_all | solution.py:14
  167.6 0.0 copy-start.2
  167.6 0.2 reduce_sum.44
  167.9 0.1 copy.29
  168.0 0.7 reshape.104
  168.7 9.7 %all-to-all-start.2 = ((bf16[24,2,512]{2,1,0:T(2,128)(2,1)}), bf16[24,2,512]{2,1,0:T(2,128)(2,1)S(1)}, u32[]{:S(2)}, u32[]{:S(2)}) async-start(bf16[24,2,512]{2,1,0:T(2,128)(2,1)} %reshape.104), calls=%async_computation.2 | async-start | bytes 98304 | tf_op jit(solution)/shard_map/all_to_all | solution.py:52
  178.5 0.0 copy-done.2
  178.5 0.1 copy.23
  178.6 9.9 %all-to-all-done.2 = bf16[24,2,512]{2,1,0:T(2,128)(2,1)S(1)} async-done(((bf16[24,2,512]{2,1,0:T(2,128)(2,1)}), bf16[24,2,512]{2,1,0:T(2,128)(2,1)S(1)}, u32[]{:S(2)}, u32[]{:S(2)}) %all-to-all-start.2) | async-done | bytes 49184 | tf_op jit(solution)/shard_map/all_to_all | solution.py:52
  188.5 0.1 reshape.105
  188.7 1.9 gather_fusion
  190.6 0.3 multiply_reduce_fusion
  190.8 0.7 copy.30
  (6 shorter events, 0.1 us)
Async XLA Ops:
  0.0 115.8 %copy-start = (bf16[1,384,2048]{2,1,0:T(8,128)(2,1)S(1)}, bf16[1,384,2048]{2,1,0:T(8,128)(2,1)}, u32[]{:S(2)}) copy-start(bf16[1,384,2048]{2,1,0:T(8,128)(2,1)} %param.13) | copy-start | bytes 4718596
  40.1 73.9 %copy-start.3 = (bf16[1,2048,384]{2,1,0:T(8,128)(2,1)S(1)}, bf16[1,2048,384]{2,1,0:T(8,128)(2,1)}, u32[]{:S(2)}) copy-start(bf16[1,2048,384]{2,1,0:T(8,128)(2,1)} %param.11) | copy-start | bytes 4718596
  112.8 1.2 copy-start.1
  167.6 10.8 %copy-start.2 = (f32[128,2]{0,1:T(2,128)S(1)}, f32[128,2]{0,1:T(2,128)}, u32[]{:S(2)}) copy-start(f32[128,2]{0,1:T(2,128)} %param.10) | copy-start | bytes 3076
  168.7 19.8 %all-to-all-start.2 = ((bf16[24,2,512]{2,1,0:T(2,128)(2,1)}), bf16[24,2,512]{2,1,0:T(2,128)(2,1)S(1)}, u32[]{:S(2)}, u32[]{:S(2)}) async-start(bf16[24,2,512]{2,1,0:T(2,128)(2,1)} %reshape.104), calls=%async_computation.2 | async-start | bytes 98304 | tf_op jit(solution)/shard_map/all_to_all | solution.py:52
where the time goes:
time: 193 us; the launch traced here: 192 us
  blocking collectives  119 us (62%)
  local copies, waits for them, and re-layouts  43.3 us (22%)
  waiting for transfers between devices  9.93 us (5%)
  starting transfers between devices  9.73 us (5%)
  matrix products  5.64 us (3%)
  other arithmetic  3.72 us (2%)
    all_to_all x1, blocking collectives, local(): lax.all_to_all(outgoing, 'ep', split_axis=0, concat_axis=0, tiled=True)  72.7 us
    all_to_all x1, blocking collectives, sent_and_summed(): lax.all_to_all(cut_along(array, dim, devices), axis, 0, 0, tiled=True)  46.4 us
    scatter x1, local copies, waits for them, and re-layouts, local(): outgoing = jnp.zeros((ep_count, capacity, width), jnp.bfloat16).at[route_...  33.3 us
    all_to_all x1, waiting for transfers between devices, local(): lax.all_to_all(back.astype(jnp.bfloat16), 'ep', split_axis=0, concat_axis...  9.93 us
    all_to_all x1, starting transfers between devices, local(): lax.all_to_all(back.astype(jnp.bfloat16), 'ep', split_axis=0, concat_axis...  9.73 us
  transfers between devices with their start and end apart: 1, of which 1 were waited for; matrix products, arithmetic and copies ran while one was open for 0% of the time, Pallas kernels for 0%

commit v1 on v0

v1 whole, which is shorter than its diff:
```python
import jax
import jax.numpy as jnp
from jax import lax
from jax.experimental import pallas as pl
from jax.experimental.pallas import tpu as pltpu
from jax.sharding import PartitionSpec as P

MESH = pl.DeviceIdType.MESH
NZ, NY, NX = 12, 8, 4
BF, F32 = jnp.bfloat16, jnp.float32
OFF = [0, 1, -1, 2, -2, 3, -3, 4, -4, 5, -5, 6]
GA, GB = (1, 5, 3), (6, 6, 3)
RA, RB = (7, 5, 3), (0, 7, 4)
DYS = [4, 3, -3, 2, -2, 1, -1, 0]
DXS = [2, 1, -1, 0]
WAYS = (1, -1)
N_SEND, N_TAKE = 224, 200


def part(span, way):
    start, count, cut = span
    return (start, cut) if way > 0 else (start + cut, count - cut)


def kernel(
    tok, gain, ids, wts, wg, wu, wd, out,
    x_buf, normed, z_out, near_out, wgu, wdn, acc, y_buf, comb_hi, comb_lo,
    ra_y, sa_y, za, ra_x, sa_x, rb_x, sb_x, zb, rb_y, sb_y, res, back,
    w_sem, s_sem, r_sem, b_sem,
):
    ep, tp = lax.axis_index("ep"), lax.axis_index("tp")
    z, core = lax.div(ep, 2), lax.rem(ep, 2)
    y, x = lax.div(tp, NX), lax.rem(tp, NX)
    half = lax.rem(x, 2)
    twin = tp + 1 - 2 * half

    def ym(d):
        return lax.rem(y + d + NY, NY)

    def xm(d):
        return lax.rem(x + d + NX, NX)

    def zm(d):
        return lax.rem(z + d + NZ, NZ)

    def tp_y(d):
        return ym(d) * NX + x

    def tp_x(d):
        return y * NX + xm(d)

    loads = [
        pltpu.make_async_copy(wg.at[0], wgu.at[:, pl.ds(0, 384)], w_sem.at[0]),
        pltpu.make_async_copy(wu.at[0], wgu.at[:, pl.ds(384, 384)], w_sem.at[1]),
        pltpu.make_async_copy(wd.at[0], wdn, w_sem.at[2]),
    ]
    for load in loads:
        load.start()

    barrier = pltpu.get_barrier_semaphore()

    def greet(e, t):
        pl.semaphore_signal(
            barrier, inc=1, device_id=(e, t), device_id_type=MESH
        )

    for off in OFF:
        for c in range(2):
            greet(2 * zm(off) + c, twin)
            if off != 0:
                greet(2 * zm(off) + c, tp)
    greet(2 * z + 1 - core, tp)
    for d in WAYS:
        greet(ep, tp_y(d))
    greet(ep, tp_x(2 * half - 1))

    send_places, take_places = {}, {}
    sent, sent_z = [], []

    def place(places, key):
        return places.setdefault(key, len(places))

    def arrival(key):
        return r_sem.at[place(take_places, key)]

    def message(key, src, dst, e, t, got=None):
        return pltpu.make_async_remote_copy(
            src_ref=src,
            dst_ref=dst,
            send_sem=s_sem.at[place(send_places, key)],
            recv_sem=arrival(key) if got is None else got,
            device_id=(e, t),
            device_id_type=MESH,
        )

    def send(*what):
        copy = message(*what)
        copy.start()
        sent.append(copy)

    def take(key, dst, got=None):
        pltpu.make_async_remote_copy(
            src_ref=dst,
            dst_ref=dst,
            send_sem=s_sem.at[0],
            recv_sem=arrival(key) if got is None else got,
            device_id=(ep, twin),
            device_id_type=MESH,
        ).wait_recv()

    def back_take(p, c):
        take(None, back.at[p, c], b_sem.at[2 * p + c])

    def norm_rows(i, carry):
        rows = pl.ds(pl.multiple_of(i * 16, 16), 16)
        values = tok[rows, :].astype(F32)
        mean = jnp.mean(values * values, axis=-1, keepdims=True)
        normed[rows, :] = (values * lax.rsqrt(mean + 1e-06) * gain[...]).astype(BF)
        return carry

    lax.fori_loop(0, 8, norm_rows, 0)

    lanes = lax.broadcasted_iota(jnp.int32, (128, 128), 1)
    rows = lax.broadcasted_iota(jnp.int32, (128, 128), 0)
    earlier = (rows < lanes).astype(F32).astype(BF)
    expert = lax.broadcasted_iota(jnp.int32, (32, 128), 0)
    id_rows = [ids[0:1, :], ids[1:2, :]]
    named = [(r == expert).astype(F32) for r in id_rows]
    before = jnp.dot((named[0] + named[1]).astype(BF), earlier, preferred_element_type=F32)
    pos = []
    for r, n in zip(id_rows, named):
        slot = jnp.sum(n * before, axis=0, keepdims=True).astype(jnp.int32)
        d = z - lax.shift_right_logical(r, 1)
        d = jnp.where(d < 0, d + NZ, d)
        tile = jnp.where(d == 0, 0, jnp.where(d <= 6, 2 * d - 1, 2 * (NZ - d)))
        pos.append(tile * 32 + (r & 1) * 16 + slot)
    row = lax.broadcasted_iota(jnp.int32, (384, 128), 0)
    at = [(p == row) for p in pos]
    pick = (at[0] | at[1]).astype(F32).astype(BF)

    column = pl.ds(pl.multiple_of(lax.div(tp, 2) * 128, 128), 128)
    rows_out = jnp.dot(pick, normed[:, column], preferred_element_type=F32)
    z_out[...] = rows_out.astype(BF).reshape(NZ, 2, 16, 128)

    pl.semaphore_wait(barrier, 24 + 22 + 1 + 2 + 1)

    for p in range(11, 0, -1):
        for c in range(2):
            sent_z.append(
                message(("z", p, c), z_out.at[p, c], x_buf.at[y, x, p],
                        2 * zm(-OFF[p]) + c, tp, arrival(("z", p)))
            )

    @pl.when(core == half)
    def _():
        for copy in sent_z:
            copy.start()

    row16 = lax.broadcasted_iota(jnp.int32, (16, 128), 0)
    for c in range(2):
        whose = core if c == 0 else 1 - core
        mine = ((pos[0] == row16 + whose * 16) | (pos[1] == row16 + whose * 16))
        near = jnp.dot(mine.astype(F32).astype(BF), normed[...], preferred_element_type=F32)
        near = near.astype(BF)
        for t in range(16):
            tile = near[:, t * 128 : (t + 1) * 128]
            if c == 0:
                x_buf[t // 2, 2 * (t % 2) + core, 0] = tile
            else:
                near_out[t % 2, t // 2] = tile
    for i in range(2):
        send(("near", i), near_out.at[i], x_buf.at[:, 2 * i + core, 0], 2 * z + 1 - core, tp)

    comb = jnp.where(at[0], wts[0:1, :], 0.0) + jnp.where(at[1], wts[1:2, :], 0.0)
    comb = jnp.transpose(comb)
    high = comb.astype(BF)
    comb_hi[...] = high
    comb_lo[...] = (comb - high.astype(F32)).astype(BF)

    def tiles(yy, xx, span):
        return x_buf.at[yy, xx, pl.ds(span[0], span[1])]

    def z_take(span):
        for p in range(span[0], span[0] + span[1]):
            take(("z", p), x_buf.at[y, x, p])

    def gax(step):
        for w in WAYS:
            if step == 1:
                send(("ax1", w), tiles(y, x, GA), tiles(y, x, GA), ep, tp_x(w))
            else:
                take(("ax1", w), tiles(y, xm(-w), GA))
                s = part(GA, w)
                send(("ax2", w), tiles(y, xm(-w), s), tiles(y, xm(-w), s), ep, tp_x(w))

    def gax_end():
        for w in WAYS:
            take(("ax2", w), tiles(y, xm(2), part(GA, w)))

    def gay(step, dx):
        xx = xm(dx)
        for w in WAYS:
            if step > 1:
                take(("ay", step - 1, dx, w), tiles(ym(-w * (step - 1)), xx, GA))
            s = part(GA, w) if step == 4 else GA
            src = tiles(ym(-w * (step - 1)), xx, s)
            send(("ay", step, dx, w), src, src, ep, tp_y(w))

    def gay_end(dx):
        for w in WAYS:
            take(("ay", 4, dx, w), tiles(ym(4), xm(dx), part(GA, w)))

    def gby(step):
        for w in WAYS:
            if step > 1:
                take(("by", step - 1, w), tiles(ym(-w * (step - 1)), x, GB))
            s = part(GB, w) if step == 4 else GB
            src = tiles(ym(-w * (step - 1)), x, s)
            send(("by", step, w), src, src, ep, tp_y(w))

    def gby_end():
        for w in WAYS:
            take(("by", 4, w), tiles(ym(4), x, part(GB, w)))

    def gbx(step, dy):
        yy = ym(dy)
        for w in WAYS:
            if step == 1:
                send(("bx1", dy, w), tiles(yy, x, GB), tiles(yy, x, GB), ep, tp_x(w))
            elif step == 2:
                take(("bx1", dy, w), tiles(yy, xm(-w), GB))
                s = part(GB, w)
                src = tiles(yy, xm(-w), s)
                send(("bx2", dy, w), src, src, ep, tp_x(w))
            else:
                take(("bx2", dy, w), tiles(yy, xm(2), part(GB, w)))

    def up(dy):
        yy = ym(dy)
        weights = wgu[pl.ds(pl.multiple_of(yy * 256, 256), 256), :]
        left = jnp.concatenate(
            [
                jnp.concatenate(
                    [x_buf[yy, h].reshape(192, 128), x_buf[yy, 2 + h].reshape(192, 128)],
                    axis=1,
                )
                for h in range(2)
            ],
            axis=0,
        )
        term = jnp.dot(left, weights, preferred_element_type=F32)
        acc[...] = term if dy == 0 else acc[...] + term

    z_take(GA)
    gax(1)
    gay(1, 0)
    gax(2)
    gay(1, 1)
    gay(1, -1)
    z_take(GB)
    gby(1)
    gbx(1, 0)
    gay(2, 0)
    gax_end()
    gay(1, 2)
    gay(2, 1)
    gay(2, -1)
    gby(2)
    gbx(2, 0)
    gbx(1, 1)
    gbx(1, -1)
    gay(3, 0)
    gay(2, 2)
    gay(3, 1)
    gay(3, -1)
    gby(3)
    gbx(3, 0)
    gbx(2, 1)
    gbx(2, -1)
    gbx(1, 2)
    gbx(1, -2)
    gay(4, 0)
    gay(3, 2)
    for i in range(2):
        take(("near", i), x_buf.at[:, 2 * i + 1 - core, 0])
    loads[0].wait()
    loads[1].wait()
    up(0)
    gby(4)
    gay(4, 1)
    gay(4, -1)
    gbx(3, 1)
    gbx(3, -1)
    gbx(2, 2)
    gbx(2, -2)
    gbx(1, 3)
    gbx(1, -3)
    gay(4, 2)
    gby_end()
    gbx(1, 4)
    up(1)
    up(-1)
    gbx(2, 3)
    gbx(2, -3)
    gbx(3, 2)
    gbx(3, -2)
    up(2)
    gbx(2, 4)
    up(-2)
    gbx(3, 3)
    gbx(3, -3)
    up(3)
    up(-3)
    for dx in (0, 1, -1, 2):
        gay_end(dx)
    gbx(3, 4)
    up(4)

    gate, upv = acc[:, :384], acc[:, 384:]
    hidden = (gate / (1.0 + jnp.exp(-gate)) * upv).astype(BF)
    loads[2].wait()

    def down(dy):
        yy = ym(dy)
        cols = pl.ds(pl.multiple_of(yy * 256, 256), 256)
        term = jnp.dot(hidden, wdn[:, cols], preferred_element_type=F32).astype(BF)
        for xx in range(NX):
            h, t = xx % 2, xx // 2
            block = term[192 * h : 192 * (h + 1), 128 * t : 128 * (t + 1)]
            y_buf[yy, xx] = block.reshape(NZ, 16, 128)

    def own(yy, xx, span):
        return y_buf[yy, xx, pl.ds(span[0], span[1])].astype(F32)

    def local(span, w):
        s = part(span, w)
        return pl.ds(s[0] - span[0], s[1])

    def whole(span):
        return pl.ds(0, span[1])

    def other(span, w):
        return local(span, -w)

    def ray(step):
        for dx in DXS:
            i = DXS.index(dx)
            for w in WAYS:
                d = 0 if w > 0 else 1
                yy = ym(w * (5 - step))
                if step == 1:
                    src = y_buf.at[yy, xm(dx), pl.ds(*part(RA, w))]
                    send(("ray", 1, dx, w), src, ra_y.at[d, 0, i, local(RA, w)], ep, tp_y(w))
                    continue
                if step == 2:
                    got = ra_y.at[d, 0, i, local(RA, w)]
                    take(("ray", 1, dx, w), got)
                    sa_y[d, 0, i, local(RA, w)] = (own(yy, xm(dx), part(RA, w)) + got[...].astype(F32)).astype(BF)
                    sa_y[d, 0, i, other(RA, w)] = y_buf[yy, xm(dx), pl.ds(*part(RA, -w))]
                else:
                    got = ra_y.at[d, step - 2, i]
                    take(("ray", step - 1, dx, w), got)
                    sa_y[d, step - 2, i] = (own(yy, xm(dx), RA) + got[...].astype(F32)).astype(BF)
                send(("ray", step, dx, w), sa_y.at[d, step - 2, i], ra_y.at[d, step - 1, i], ep, tp_y(w))

    def ray_end(dx):
        i = DXS.index(dx)
        total = own(y, xm(dx), RA)
        for w in WAYS:
            d = 0 if w > 0 else 1
            take(("ray", 4, dx, w), ra_y.at[d, 3, i])
            total = total + ra_y[d, 3, i].astype(F32)
        za[i] = total.astype(BF)

    def rax(step):
        for w in WAYS:
            d = 0 if w > 0 else 1
            here = local(RA, w)
            if step == 1:
                send(("rax", 1, w), za.at[0, here], ra_x.at[d, 0, here], ep, tp_x(w))
            else:
                got = ra_x.at[d, 0, here]
                take(("rax", 1, w), got)
                i = DXS.index(w)
                sa_x[d, here] = (za[i, here].astype(F32) + got[...].astype(F32)).astype(BF)
                sa_x[d, other(RA, w)] = za[i, other(RA, w)]
                send(("rax", 2, w), sa_x.at[d], ra_x.at[d, 1], ep, tp_x(w))

    def rax_end():
        total = za[3].astype(F32)
        for w in WAYS:
            d = 0 if w > 0 else 1
            take(("rax", 2, w), ra_x.at[d, 1])
            total = total + ra_x[d, 1].astype(F32)
        res[pl.ds(RA[0], RA[1])] = total.astype(BF)

    def rbx(step, dy):
        i, yy = DYS.index(dy), ym(dy)
        for w in WAYS:
            d = 0 if w > 0 else 1
            here = local(RB, w)
            if step == 1:
                src = y_buf.at[yy, xm(2), pl.ds(*part(RB, w))]
                send(("rbx", 1, dy, w), src, rb_x.at[i, d, 0, here], ep, tp_x(w))
            elif step == 2:
                got = rb_x.at[i, d, 0, here]
                take(("rbx", 1, dy, w), got)
                sb_x[i, d, here] = (own(yy, xm(w), part(RB, w)) + got[...].astype(F32)).astype(BF)
                sb_x[i, d, other(RB, w)] = y_buf[yy, xm(w), pl.ds(*part(RB, -w))]
                send(("rbx", 2, dy, w), sb_x.at[i, d], rb_x.at[i, d, 1], ep, tp_x(w))
        if step == 3:
            total = own(yy, x, RB)
            for w in WAYS:
                d = 0 if w > 0 else 1
                take(("rbx", 2, dy, w), rb_x.at[i, d, 1])
                total = total + rb_x[i, d, 1].astype(F32)
            zb[i] = total.astype(BF)

    def rby(step):
        for w in WAYS:
            d = 0 if w > 0 else 1
            here = local(RB, w)
            if step == 1:
                send(("rby", 1, w), zb.at[0, here], rb_y.at[d, 0, here], ep, tp_y(w))
                continue
            i = DYS.index(w * (5 - step))
            if step == 2:
                got = rb_y.at[d, 0, here]
                take(("rby", 1, w), got)
                sb_y[d, 0, here] = (zb[i, here].astype(F32) + got[...].astype(F32)).astype(BF)
                sb_y[d, 0, other(RB, w)] = zb[i, other(RB, w)]
            else:
                take(("rby", step - 1, w), rb_y.at[d, step - 2])
                sb_y[d, step - 2] = (zb[i].astype(F32) + rb_y[d, step - 2].astype(F32)).astype(BF)
            send(("rby", step, w), sb_y.at[d, step - 2], rb_y.at[d, step - 1], ep, tp_y(w))

    def rby_end():
        total = zb[7].astype(F32)
        for w in WAYS:
            d = 0 if w > 0 else 1
            take(("rby", 4, w), rb_y.at[d, 3])
            total = total + rb_y[d, 3].astype(F32)
        res[pl.ds(RB[0], RB[1])] = total.astype(BF)

    for dy in DYS:
        down(dy)
        if dy == 4:
            ray(1)
        rbx(1, dy)
    ray(2)
    for dy in DYS[:3]:
        rbx(2, dy)
    ray(3)
    for dy in DYS[3:]:
        rbx(2, dy)
    rbx(3, 4)
    rby(1)
    ray(4)
    rbx(3, 3)
    rbx(3, -3)
    rby(2)
    ray_end(2)
    rax(1)
    ray_end(1)
    ray_end(-1)
    rbx(3, 2)
    rbx(3, -2)
    rby(3)
    rax(2)
    ray_end(0)
    rbx(3, 1)
    rbx(3, -1)
    rby(4)

    def give(span):
        for p in range(span[0] + span[1] - 1, span[0] - 1, -1):
            e, got = 2 * zm(OFF[p]) + half, b_sem.at[2 * p + core]
            send(("back", p, 1), res.at[p], back.at[p, core], e, twin, got)
            if p > 0:
                send(("back", p, 0), res.at[p], back.at[p, core], e, tp, got)

    rax_end()
    give(RA)
    rbx(3, 0)
    rby_end()
    give(RB)
    near_back = message(
        ("back", 0, 0), res.at[0], back.at[0, core], 2 * z + half, tp, b_sem.at[core]
    )

    @pl.when(half == core)
    def _():
        back[0, core] = res[0]

    @pl.when(half != core)
    def _():
        near_back.start()

    for p in range(11, 0, -1):
        for c in range(2):
            back_take(p, c)
    back_take(0, 1 - core)

    @pl.when(half != core)
    def _():
        back_take(0, core)
        near_back.wait_send()

    rows_in = back[...].reshape(384, 128)
    mixed = jnp.dot(comb_hi[...], rows_in, preferred_element_type=F32)
    mixed = mixed + jnp.dot(comb_lo[...], rows_in, preferred_element_type=F32)
    mixed = jnp.where(half == 1, pltpu.roll(mixed, 64, 1), mixed)
    out[...] = mixed[:, :64].astype(BF)

    for copy in sent:
        copy.wait_send()

    @pl.when(core == half)
    def _():
        for copy in sent_z:
            copy.wait_send()


def per_device(tokens, norm_gain, route_ids, route_weights, gate_proj, up_proj, down_proj):
    vmem = pl.BlockSpec(memory_space=pltpu.VMEM)
    hbm = pl.BlockSpec(memory_space=pl.ANY)

    def tiles(*lead):
        return pltpu.VMEM((*lead, 16, 128), BF)

    a, b = RA[1], RB[1]
    return pl.pallas_call(
        kernel,
        out_shape=jax.ShapeDtypeStruct((128, 64), BF),
        in_specs=[vmem] * 4 + [hbm] * 3,
        out_specs=vmem,
        scratch_shapes=[
            tiles(NY, NX, NZ),
            pltpu.VMEM((128, 2048), BF),
            tiles(NZ, 2),
            tiles(2, NY),
            pltpu.VMEM((2048, 768), BF),
            pltpu.VMEM((384, 2048), BF),
            pltpu.VMEM((384, 768), F32),
            tiles(NY, NX, NZ),
            pltpu.VMEM((128, 384), BF),
            pltpu.VMEM((128, 384), BF),
            tiles(2, 4, 4, a), tiles(2, 3, 4, a), tiles(4, a), tiles(2, 2, a), tiles(2, a),
            tiles(8, 2, 2, b), tiles(8, 2, b), tiles(8, b), tiles(2, 4, b), tiles(2, 3, b),
            tiles(NZ),
            tiles(NZ, 2),
            pltpu.SemaphoreType.DMA((3,)),
            pltpu.SemaphoreType.DMA((N_SEND,)),
            pltpu.SemaphoreType.DMA((N_TAKE,)),
            pltpu.SemaphoreType.DMA((2 * NZ,)),
        ],
        compiler_params=pltpu.CompilerParams(collective_id=0, has_side_effects=True),
        cost_estimate=pl.CostEstimate(
            flops=2_000_000_000, bytes_accessed=6_000_000, transcendentals=200_000
        ),
    )(
        tokens, norm_gain.reshape(1, -1), route_ids.T, route_weights.T,
        gate_proj, up_proj, down_proj,
    )


def solution(mesh):
    placed = (
        P("ep", None),
        P(),
        P("ep", None),
        P("ep", None),
        P("ep", None, "tp"),
        P("ep", None, "tp"),
        P("ep", "tp", None),
    )
    return jax.shard_map(
        per_device, mesh=mesh, in_specs=placed, out_specs=P("ep", "tp"), check_vma=False
    )
```

time: 193 us -> 81.4 us (0.42)
  blocking collectives: 119 us -> 0 us
  Pallas kernels: 0 us -> 79.8 us
  local copies, waits for them, and re-layouts: 43.3 us -> 1.45 us
  waiting for transfers between devices: 9.93 us -> 0 us
  starting transfers between devices: 9.73 us -> 0 us
  matrix products: 5.64 us -> 0 us
  other arithmetic: 3.72 us -> 0 us
    all_to_all x2 -> x0, blocking collectives: 119 us -> none  [the longest x1 72.7 us: local(): lax.all_to_all(outgoing, 'ep', split_axis=0, concat_axis=0, tiled=True)]
    pallas_call x0 -> x1, Pallas kernels: none -> 79.8 us  [per_device(): pl.pallas_call(kernel, out_shape=jax.ShapeDtypeStruct((128, 64), BF), in_...]
    scatter x1 -> x0, local copies, waits for them, and re-layouts: 33.3 us -> none  [local(): outgoing = jnp.zeros((ep_count, capacity, width), jnp.bfloat16).at[route_...]
    all_to_all x1 -> x0, waiting for transfers between devices: 9.93 us -> none  [local(): lax.all_to_all(back.astype(jnp.bfloat16), 'ep', split_axis=0, concat_axis...]
    all_to_all x1 -> x0, starting transfers between devices: 9.73 us -> none  [local(): lax.all_to_all(back.astype(jnp.bfloat16), 'ep', split_axis=0, concat_axis...]
    dot_general x2 -> x0, matrix products: 5.64 us -> none  [the longest x1 3.85 us: local(): lax.dot_general(down_local, hidden, (((0,), (1,)), ((), ())), preferred_e...]
    unnamed x12 -> x0, local copies, waits for them, and re-layouts: 3.05 us -> none
  transfers between devices with their start and end apart: 1 -> 0, of which waited for: 1 -> 0; matrix products, arithmetic and copies ran while one was open for 0% -> 0% of each run, Pallas kernels for 0% -> 0%
where the time goes in v1:
time: 81.4 us; the launch traced here: 81.2 us
  Pallas kernels  79.8 us (98%)
  local copies, waits for them, and re-layouts  1.45 us (2%)
    pallas_call x1, Pallas kernels, per_device(): pl.pallas_call(kernel, out_shape=jax.ShapeDtypeStruct((128, 64), BF), in_...  79.8 us

profile of v1, /device:TPU:1, one launch (start us, length us, event | category | flops | bytes accessed | tf_op | source)
XLA Modules:
  0.0 81.2 jit_solution(4394238019164685935)
XLA Ops:
  0.0 79.8 %shard_map.73 = bf16[128,64]{1,0:T(8,128)(2,1)} custom-call(bf16[128,2048]{1,0:T(8,128)(2,1)} %tok.1, f32[1,2048]{1,0:T(1,128)} %bitcast.3, s32[2,128]{1,0:T(2,128)} %bitcast.4, f32[2,128]{1,0:T(2,128)} %bitcast.5, bf16[1,2048,384]{2,1,0:T(8,128)(2,1)} %wg.1, bf16[1,2048,384]{2,1,0:T(8,128)(2,1)} %wu.1, bf16[1,384,2048]{2,1,0:T(8,128)(2,1)} %wd.1), custom_call_target="tpu_custom_call" | custom-call | flops 2000000000 | bytes 6000000 | tf_op jit(solution)/shard_map/pallas_call | solution.py:532
  79.8 1.4 %copy.8 = bf16[128,64]{0,1:T(8,128)(2,1)} copy(bf16[128,64]{1,0:T(8,128)(2,1)} %shard_map.73) | data formatting | bytes 32768 | tf_op jit(solution)/shard_map/pallas_call | solution.py:532

commit v2 on v0

v2 whole, which is shorter than its diff:
```python
import jax
import jax.numpy as jnp
from jax import lax
from jax.experimental import pallas as pl
from jax.experimental.pallas import tpu as pltpu
from jax.sharding import PartitionSpec as P

MESH = pl.DeviceIdType.MESH
NZ, NY, NX = 12, 8, 4
BF, F32 = jnp.bfloat16, jnp.float32
OFF = [0, 1, -1, 2, -2, 3, -3, 4, -4, 5, -5, 6]
RA, RB = (0, 6, 3), (6, 6, 3)
NEAR = [(1, 2), (3, 2), (5, 1)]
FAR, LAST = (6, 3), (9, 3)
DYS = [4, 3, -3, 2, -2, 1, -1, 0]
DXS = [2, 1, -1, 0]
WAYS = (1, -1)
N_TAKE, POOL = 109, 2048


def part(span, way):
    start, count, cut = span
    return (start, cut) if way > 0 else (start + cut, count - cut)


def kernel(
    tok_in, gain_in, ids_in, wts_in, wg, wu, wd, out,
    tok, gain, ids, wts, x_buf, normed, z_near, z_far, near_out, wgu, wdn, acc, y_buf, comb_hi, comb_lo,
    ra_y, sa_y, za, ra_x, rb_x, sb_x, zb, rb_y, res, back,
    pool, w_sem, s_sem, r_sem,
):
    ep, tp = lax.axis_index("ep"), lax.axis_index("tp")
    z, core = lax.div(ep, 2), lax.rem(ep, 2)
    y, x = lax.div(tp, NX), lax.rem(tp, NX)
    half = lax.rem(x, 2)
    twin = tp + 1 - 2 * half

    def ym(d):
        return lax.rem(y + d + NY, NY)

    def xm(d):
        return lax.rem(x + d + NX, NX)

    def zm(d):
        return lax.rem(z + d + NZ, NZ)

    def tp_y(d):
        return ym(d) * NX + x

    def tp_x(d):
        return y * NX + xm(d)

    barrier = pltpu.get_barrier_semaphore()

    def greet(e, t):
        pl.semaphore_signal(barrier, inc=1, device_id=(e, t), device_id_type=MESH)

    for off in OFF[::-1]:
        for c in range(2):
            greet(2 * zm(off) + c, twin)
            if off != 0:
                greet(2 * zm(off) + c, tp)
    greet(2 * z + 1 - core, tp)
    for d in DYS[:-1]:
        greet(ep, tp_y(d))
    greet(ep, tp_x(2))
    greet(ep, tp_x(2 * half - 1))

    loads = [
        pltpu.make_async_copy(tok_in, tok, w_sem.at[0]),
        pltpu.make_async_copy(gain_in, gain, w_sem.at[1]),
        pltpu.make_async_copy(ids_in, ids, w_sem.at[2]),
        pltpu.make_async_copy(wts_in, wts, w_sem.at[3]),
        pltpu.make_async_copy(wg.at[0], wgu.at[:, pl.ds(0, 384)], w_sem.at[4]),
        pltpu.make_async_copy(wu.at[0], wgu.at[:, pl.ds(384, 384)], w_sem.at[5]),
        pltpu.make_async_copy(wd.at[0], wdn, w_sem.at[6]),
    ]
    for load in loads:
        load.start()

    places = {}
    sent, sent_z = [], []

    def arrival(key):
        return r_sem.at[places.setdefault(key, len(places))]

    def message(key, src, dst, e, t, group=0):
        return pltpu.make_async_remote_copy(
            src_ref=src,
            dst_ref=dst,
            send_sem=s_sem.at[group],
            recv_sem=arrival(key),
            device_id=(e, t),
            device_id_type=MESH,
        )

    def count(ref):
        size = 1
        for n in ref.shape:
            size *= n
        return size // 2048

    def send(key, src, dst, e, t):
        message(key, src, dst, e, t).start()
        sent.append(count(src))

    def take(key, dst):
        pltpu.make_async_remote_copy(
            src_ref=dst,
            dst_ref=dst,
            send_sem=s_sem.at[0],
            recv_sem=arrival(key),
            device_id=(ep, twin),
            device_id_type=MESH,
        ).wait_recv()

    def wait_sent(group, tiles):
        ref = pool.at[pl.ds(0, tiles)]
        pltpu.make_async_remote_copy(
            src_ref=ref,
            dst_ref=ref,
            send_sem=s_sem.at[group],
            recv_sem=r_sem.at[0],
            device_id=(ep, twin),
            device_id_type=MESH,
        ).wait_send()

    for load in loads[:4]:
        load.wait()

    def norm_rows(i, carry):
        rows = pl.ds(pl.multiple_of(i * 16, 16), 16)
        values = tok[rows, :].astype(F32)
        mean = jnp.mean(values * values, axis=-1, keepdims=True)
        normed[rows, :] = (values * lax.rsqrt(mean + 1e-06) * gain[...]).astype(BF)
        return carry

    lax.fori_loop(0, 8, norm_rows, 0)

    lanes = lax.broadcasted_iota(jnp.int32, (128, 128), 1)
    rows = lax.broadcasted_iota(jnp.int32, (128, 128), 0)
    earlier = (rows < lanes).astype(F32).astype(BF)
    expert = lax.broadcasted_iota(jnp.int32, (32, 128), 0)
    id_rows = [ids[0:1, :], ids[1:2, :]]
    named = [(r == expert).astype(F32) for r in id_rows]
    before = jnp.dot((named[0] + named[1]).astype(BF), earlier, preferred_element_type=F32)
    pos = []
    for r, n in zip(id_rows, named):
        slot = jnp.sum(n * before, axis=0, keepdims=True).astype(jnp.int32)
        d = z - lax.shift_right_logical(r, 1)
        d = jnp.where(d < 0, d + NZ, d)
        tile = jnp.where(d == 0, 0, jnp.where(d <= 6, 2 * d - 1, 2 * (NZ - d)))
        pos.append(tile * 32 + (r & 1) * 16 + slot)
    row = lax.broadcasted_iota(jnp.int32, (384, 128), 0)
    at = [(p == row) for p in pos]
    pick = (at[0] | at[1]).astype(F32).astype(BF)

    pair = lax.div(x, 2)
    column = pl.ds(pl.multiple_of(y * 256, 256), 256)
    rows_out = jnp.dot(pick[32:192], normed[:, column], preferred_element_type=F32)
    for t in range(2):
        z_near[:, :, t] = rows_out[:, 128 * t : 128 * (t + 1)].astype(BF).reshape(5, 2, 16, 128)
    for yy in range(NY):
        column = pl.ds(pl.multiple_of((2 * yy + pair) * 128, 128), 128)
        rows_out = jnp.dot(pick[192:], normed[:, column], preferred_element_type=F32)
        z_far[:, :, yy] = rows_out.astype(BF).reshape(6, 2, 16, 128)

    pl.semaphore_wait(barrier, 24 + 22 + 1 + 7 + 2)

    for p in range(1, 6):
        for c in range(2):
            send(("zn", (p - 1) // 2), z_near.at[p - 1, c], x_buf.at[y, :, core, p],
                 2 * zm(-OFF[p]) + c, tp)
    for p in (11, 10, 9, 8, 7, 6):
        for c in range(2):
            src, dst = z_far.at[p - 6, c], x_buf.at[:, pair, half, p]
            if p >= LAST[0]:
                src, dst = z_far.at[p - 6, c, y], x_buf.at[y, pair, half, p]
            key = ("zl",) if p >= LAST[0] else ("zf",)
            sent_z.append((message(key, src, dst, 2 * zm(-OFF[p]) + c, tp, 1), count(src)))

    @pl.when(core == half)
    def _():
        for copy, _ in sent_z:
            copy.start()

    row16 = lax.broadcasted_iota(jnp.int32, (16, 128), 0)
    for c in range(2):
        whose = core if c == 0 else 1 - core
        mine = ((pos[0] == row16 + whose * 16) | (pos[1] == row16 + whose * 16))
        near = jnp.dot(mine.astype(F32).astype(BF), normed[...], preferred_element_type=F32)
        near = near.astype(BF)
        for t in range(16):
            tile = near[:, t * 128 : (t + 1) * 128]
            if c == 0:
                x_buf[t // 2, t % 2, core, 0] = tile
            else:
                near_out[t // 2, t % 2] = tile
    send(("near",), near_out, x_buf.at[:, :, core, 0], 2 * z + 1 - core, tp)

    comb = jnp.where(at[0], wts[0:1, :], 0.0) + jnp.where(at[1], wts[1:2, :], 0.0)
    comb = jnp.transpose(comb)
    high = comb.astype(BF)
    comb_hi[...] = high
    comb_lo[...] = (comb - high.astype(F32)).astype(BF)

    def gather_y(chunk, step):
        ps = pl.ds(*NEAR[chunk])
        if step == 1:
            take(("zn", chunk), x_buf.at[y, :, :, ps])
        if step == 5:
            take(("gy", chunk, 4), x_buf.at[ym(4), :, :, ps])
            return
        for w in WAYS:
            yy = ym(-w * (step - 1))
            if step > 1:
                take(("gy", chunk, step - 1, w), x_buf.at[yy, :, :, ps])
            src = x_buf.at[yy, :, :, ps]
            if step == 4:
                src = x_buf.at[yy, 0 if w > 0 else 1, :, ps]
            key = ("gy", chunk, step) if step == 4 else ("gy", chunk, step, w)
            send(key, src, src, ep, tp_y(w))

    def column_of(rows, xx, ps):
        return x_buf.at[rows, lax.div(xx, 2), lax.rem(xx, 2), ps]

    def gather_x(step):
        ps = pl.ds(*FAR)
        if step == 1:
            take(("zf",), x_buf.at[:, pair, half, ps])
        if step == 3:
            take(("gx", 2), column_of(pl.ds(0, 8), xm(2), ps))
            return
        for w in WAYS:
            part_y = pl.ds(0 if w > 0 else 4, 4)
            xx = xm(-w * (step - 1))
            rows = pl.ds(0, 8)
            if step == 2:
                take(("gx", 1, w), column_of(rows, xx, ps))
                rows = part_y
            src = column_of(rows, xx, ps)
            send(("gx", step, w) if step == 1 else ("gx", 2), src, src, ep, tp_x(w))

    def last_y():
        src = x_buf.at[y, pair, half, pl.ds(*LAST)]
        take(("zl",), src)
        for dy in DYS[:7]:
            send(("ly", dy), src, src, ep, tp_y(dy))

    def last_x(step, *dys):
        if step == 3:
            take(("lx2",), column_of(pl.ds(0, 8), xm(2), pl.ds(*LAST)))
        for dy in dys:
            yy, cut = ym(-dy), 1 + DYS.index(dy) % 2
            if step == 1 and dy:
                take(("ly", dy), x_buf.at[yy, pair, half, pl.ds(*LAST)])
            for w in WAYS:
                ps = pl.ds(*LAST)
                piece = pl.ds(*part((*LAST, cut), w))
                xx = xm(-w * (step - 1))
                if step == 2:
                    take(("lx1", dy, w), column_of(yy, xx, ps))
                    ps = piece
                src = column_of(yy, xx, ps)
                send(("lx1", dy, w) if step == 1 else ("lx2",), src, src, ep, tp_x(w))

    def up(yy, first, start):
        weights = wgu[pl.ds(pl.multiple_of(yy * 256, 256), 256), :]
        ps = pl.ds(first, 6)
        left = jnp.concatenate(
            [
                jnp.concatenate(
                    [x_buf[yy, t, h, ps].reshape(96, 128) for t in range(2)], axis=1
                )
                for h in range(2)
            ],
            axis=0,
        )
        term = jnp.dot(left, weights, preferred_element_type=F32)
        acc[...] = term if start else acc[...] + term

    def act():
        gate, upv = acc[:, :384], acc[:, 384:]
        return (gate / (1.0 + jnp.exp(-gate)) * upv).astype(BF)

    def down(hidden, dy, first):
        yy = ym(dy)
        cols = pl.ds(pl.multiple_of(yy * 256, 256), 256)
        term = jnp.dot(hidden, wdn[:, cols], preferred_element_type=F32).astype(BF)
        for xx in range(NX):
            h, t = xx % 2, xx // 2
            block = term[96 * h : 96 * (h + 1), 128 * t : 128 * (t + 1)]
            y_buf[yy, xx, pl.ds(first, 6)] = block.reshape(6, 16, 128)

    def own(yy, xx, span):
        return y_buf[yy, xx, pl.ds(span[0], span[1])].astype(F32)

    def local(span, w):
        s = part(span, w)
        return pl.ds(s[0] - span[0], s[1])

    def whole(span):
        return pl.ds(0, span[1])

    def other(span, w):
        return local(span, -w)

    def ray(step):
        for dx in DXS:
            i = DXS.index(dx)
            for w in WAYS:
                d = 0 if w > 0 else 1
                yy = ym(w * (5 - step))
                if step == 1:
                    src = y_buf.at[yy, xm(dx), pl.ds(*part(RA, w))]
                    send(("ray", 1, dx, w), src, ra_y.at[d, 0, i, local(RA, w)], ep, tp_y(w))
                    continue
                if step == 2:
                    got = ra_y.at[d, 0, i, local(RA, w)]
                    take(("ray", 1, dx, w), got)
                    sa_y[d, 0, i, local(RA, w)] = (own(yy, xm(dx), part(RA, w)) + got[...].astype(F32)).astype(BF)
                    sa_y[d, 0, i, other(RA, w)] = y_buf[yy, xm(dx), pl.ds(*part(RA, -w))]
                else:
                    got = ra_y.at[d, step - 2, i]
                    take(("ray", step - 1, dx, w), got)
                    sa_y[d, step - 2, i] = (own(yy, xm(dx), RA) + got[...].astype(F32)).astype(BF)
                key = ("ray", 4, dx) if step == 4 else ("ray", step, dx, w)
                send(key, sa_y.at[d, step - 2, i], ra_y.at[d, step - 1, i], ep, tp_y(w))

    def ray_end(dx):
        i = DXS.index(dx)
        take(("ray", 4, dx), ra_y.at[:, 3, i])
        total = own(y, xm(dx), RA) + ra_y[0, 3, i].astype(F32) + ra_y[1, 3, i].astype(F32)
        za[i] = total.astype(BF)

    def rax(dx):
        i = DXS.index(dx)
        send(("rax",), za.at[i], ra_x.at[i], ep, tp_x(dx))

    def rax_end():
        total = za[3].astype(F32)
        take(("rax",), ra_x)
        for i in range(3):
            total = total + ra_x[i].astype(F32)
        res[pl.ds(RA[0], RA[1])] = total.astype(BF)

    def rbx(step, dy):
        i, yy = DYS.index(dy), ym(dy)
        for w in WAYS:
            d = 0 if w > 0 else 1
            here = local(RB, w)
            if step == 1:
                src = y_buf.at[yy, xm(2), pl.ds(*part(RB, w))]
                send(("rbx", 1, dy, w), src, rb_x.at[i, d, 0, here], ep, tp_x(w))
            elif step == 2:
                got = rb_x.at[i, d, 0, here]
                take(("rbx", 1, dy, w), got)
                sb_x[i, d, here] = (own(yy, xm(w), part(RB, w)) + got[...].astype(F32)).astype(BF)
                sb_x[i, d, other(RB, w)] = y_buf[yy, xm(w), pl.ds(*part(RB, -w))]
                send(("rbx", 2, dy), sb_x.at[i, d], rb_x.at[i, d, 1], ep, tp_x(w))
        if step == 3:
            take(("rbx", 2, dy), rb_x.at[i, :, 1])
            total = own(yy, x, RB) + rb_x[i, 0, 1].astype(F32) + rb_x[i, 1, 1].astype(F32)
            zb[i] = total.astype(BF)

            if i < 7:
                send(("rby",), zb.at[i], rb_y.at[i], ep, tp_y(dy))

    def rby_end():
        total = zb[7].astype(F32)
        take(("rby",), rb_y)
        for i in range(7):
            total = total + rb_y[i].astype(F32)
        res[pl.ds(RB[0], RB[1])] = total.astype(BF)

    for chunk in range(3):
        gather_y(chunk, 1)
    last_y()
    last_x(1, 0)
    gather_y(0, 2)
    gather_x(1)
    gather_y(1, 2)
    gather_y(2, 2)
    gather_y(0, 3)
    last_x(1, 1, -1)
    gather_y(1, 3)
    gather_y(2, 3)
    last_x(1, 2, -2)
    gather_x(2)
    gather_y(0, 4)
    last_x(1, 3, -3, 4)
    last_x(2, 0, 1, -1)
    gather_y(1, 4)
    gather_y(2, 4)
    take(("near",), x_buf.at[:, :, 1 - core, 0])
    loads[4].wait()
    loads[5].wait()
    for dy in (0, 1, -1):
        up(ym(dy), 0, dy == 0)
    last_x(2, 2, -2)
    for dy in (2, -2, 3, -3):
        up(ym(dy), 0, False)
    last_x(2, 3, -3, 4)
    for chunk in range(3):
        gather_y(chunk, 5)
    up(ym(4), 0, False)
    hidden = act()
    loads[6].wait()
    for dy in DYS:
        down(hidden, dy, 0)
        if dy == 4:
            ray(1)
    gather_x(3)
    last_x(3)
    ray(2)
    for yy in range(NY):
        up(yy, 6, yy == 0)
    hidden = act()
    for dy in DYS:
        down(hidden, dy, 6)
        rbx(1, dy)
    ray(3)
    for dy in DYS:
        rbx(2, dy)
    for dy in DYS[:3]:
        rbx(3, dy)
    ray(4)
    for dy in DYS[3:]:
        rbx(3, dy)
    for dx in DXS:
        ray_end(dx)
        if dx:
            rax(dx)

    def give(span):
        for p in range(span[0] + span[1] - 1, span[0] - 1, -1):
            e = 2 * zm(OFF[p]) + half
            send(("back",), res.at[p], back.at[p, core], e, twin)
            if p > 0:
                send(("back",), res.at[p], back.at[p, core], e, tp)

    rax_end()
    give(RA)
    rby_end()
    give(RB)
    near_back = message(("back",), res.at[0], back.at[0, core], 2 * z + half, tp, 2)

    @pl.when(half == core)
    def _():
        back[0, core] = res[0]
        take(("back",), pool.at[pl.ds(0, 23)])

    @pl.when(half != core)
    def _():
        near_back.start()
        take(("back",), pool.at[pl.ds(0, 24)])
        wait_sent(2, 1)

    rows_in = back[...].reshape(384, 128)
    mixed = jnp.dot(comb_hi[...], rows_in, preferred_element_type=F32)
    mixed = mixed + jnp.dot(comb_lo[...], rows_in, preferred_element_type=F32)
    mixed = jnp.where(half == 1, pltpu.roll(mixed, 64, 1), mixed)
    out[...] = mixed[:, :64].astype(BF)

    wait_sent(0, sum(sent))

    @pl.when(core == half)
    def _():
        wait_sent(1, sum(n for _, n in sent_z))

    assert len(places) == N_TAKE and sum(sent) <= POOL, (len(places), sum(sent))


def per_device(tokens, norm_gain, route_ids, route_weights, gate_proj, up_proj, down_proj):
    vmem = pl.BlockSpec(memory_space=pltpu.VMEM)
    hbm = pl.BlockSpec(memory_space=pl.ANY)

    def tiles(*lead):
        return pltpu.VMEM((*lead, 16, 128), BF)

    a, b = RA[1], RB[1]
    return pl.pallas_call(
        kernel,
        out_shape=jax.ShapeDtypeStruct((128, 64), BF),
        in_specs=[hbm] * 7,
        out_specs=vmem,
        scratch_shapes=[
            pltpu.VMEM((128, 2048), BF),
            pltpu.VMEM((1, 2048), F32),
            pltpu.VMEM((2, 128), jnp.int32),
            pltpu.VMEM((2, 128), F32),
            tiles(NY, 2, 2, NZ),
            pltpu.VMEM((128, 2048), BF),
            tiles(5, 2, 2),
            tiles(6, 2, NY),
            tiles(NY, 2),
            pltpu.VMEM((2048, 768), BF),
            pltpu.VMEM((384, 2048), BF),
            pltpu.VMEM((192, 768), F32),
            tiles(NY, NX, NZ),
            pltpu.VMEM((128, 384), BF),
            pltpu.VMEM((128, 384), BF),
            tiles(2, 4, 4, a), tiles(2, 3, 4, a), tiles(4, a), tiles(3, a),
            tiles(8, 2, 2, b), tiles(8, 2, b), tiles(8, b), tiles(7, b),
            tiles(NZ),
            tiles(NZ, 2),
            tiles(POOL),
            pltpu.SemaphoreType.DMA((7,)),
            pltpu.SemaphoreType.DMA((3,)),
            pltpu.SemaphoreType.DMA((N_TAKE,)),
        ],
        compiler_params=pltpu.CompilerParams(collective_id=0, has_side_effects=True),
        cost_estimate=pl.CostEstimate(
            flops=2_000_000_000, bytes_accessed=6_000_000, transcendentals=200_000
        ),
    )(
        tokens, norm_gain.reshape(1, -1), route_ids.T, route_weights.T,
        gate_proj, up_proj, down_proj,
    )


def solution(mesh):
    placed = (
        P("ep", None),
        P(),
        P("ep", None),
        P("ep", None),
        P("ep", None, "tp"),
        P("ep", None, "tp"),
        P("ep", "tp", None),
    )
    return jax.shard_map(
        per_device, mesh=mesh, in_specs=placed, out_specs=P("ep", "tp"), check_vma=False
    )
```

time: 193 us -> 70.8 us (0.37)
  blocking collectives: 119 us -> 0 us
  Pallas kernels: 0 us -> 69.1 us
  local copies, waits for them, and re-layouts: 43.3 us -> 1.45 us
  waiting for transfers between devices: 9.93 us -> 0 us
  starting transfers between devices: 9.73 us -> 0 us
  matrix products: 5.64 us -> 0 us
  other arithmetic: 3.72 us -> 0 us
    all_to_all x2 -> x0, blocking collectives: 119 us -> none  [the longest x1 72.7 us: local(): lax.all_to_all(outgoing, 'ep', split_axis=0, concat_axis=0, tiled=True)]
    pallas_call x0 -> x1, Pallas kernels: none -> 69.1 us  [per_device(): pl.pallas_call(kernel, out_shape=jax.ShapeDtypeStruct((128, 64), BF), in_...]
    scatter x1 -> x0, local copies, waits for them, and re-layouts: 33.3 us -> none  [local(): outgoing = jnp.zeros((ep_count, capacity, width), jnp.bfloat16).at[route_...]
    all_to_all x1 -> x0, waiting for transfers between devices: 9.93 us -> none  [local(): lax.all_to_all(back.astype(jnp.bfloat16), 'ep', split_axis=0, concat_axis...]
    all_to_all x1 -> x0, starting transfers between devices: 9.73 us -> none  [local(): lax.all_to_all(back.astype(jnp.bfloat16), 'ep', split_axis=0, concat_axis...]
    dot_general x2 -> x0, matrix products: 5.64 us -> none  [the longest x1 3.85 us: local(): lax.dot_general(down_local, hidden, (((0,), (1,)), ((), ())), preferred_e...]
    unnamed x12 -> x0, local copies, waits for them, and re-layouts: 3.05 us -> none
  transfers between devices with their start and end apart: 1 -> 0, of which waited for: 1 -> 0; matrix products, arithmetic and copies ran while one was open for 0% -> 0% of each run, Pallas kernels for 0% -> 0%
where the time goes in v2:
time: 70.8 us; the launch traced here: 70.6 us
  Pallas kernels  69.1 us (98%)
  local copies, waits for them, and re-layouts  1.45 us (2%)
    pallas_call x1, Pallas kernels, per_device(): pl.pallas_call(kernel, out_shape=jax.ShapeDtypeStruct((128, 64), BF), in_...  69.1 us
    pallas_call x1, local copies, waits for them, and re-layouts, per_device(): pl.pallas_call(kernel, out_shape=jax.ShapeDtypeStruct((128, 64), BF), in_...  1.45 us

profile of v2, /device:TPU:1, one launch (start us, length us, event | category | flops | bytes accessed | tf_op | source)
XLA Modules:
  0.0 70.6 jit_solution(10554707237758371718)
XLA Ops:
  0.0 69.1 %shard_map.73 = bf16[128,64]{1,0:T(8,128)(2,1)} custom-call(bf16[128,2048]{1,0:T(8,128)(2,1)} %tok_in.1, f32[1,2048]{1,0:T(1,128)} %bitcast.3, s32[2,128]{1,0:T(2,128)} %bitcast.4, f32[2,128]{1,0:T(2,128)} %bitcast.5, bf16[1,2048,384]{2,1,0:T(8,128)(2,1)} %wg.1, bf16[1,2048,384]{2,1,0:T(8,128)(2,1)} %wu.1, bf16[1,384,2048]{2,1,0:T(8,128)(2,1)} %wd.1), custom_call_target="tpu_custom_call" | custom-call | flops 2000000000 | bytes 6000000 | tf_op jit(solution)/shard_map/pallas_call | solution.py:482
  69.1 1.4 %copy.8 = bf16[128,64]{0,1:T(8,128)(2,1)} copy(bf16[128,64]{1,0:T(8,128)(2,1)} %shard_map.73) | data formatting | bytes 32768 | tf_op jit(solution)/shard_map/pallas_call | solution.py:482

commit v3 on v2

--- a/solution.py
+++ b/solution.py
@@ -12,10 +12,11 @@
 RA, RB = (0, 6, 3), (6, 6, 3)
 NEAR = [(1, 2), (3, 2), (5, 1)]
 FAR, LAST = (6, 3), (9, 3)
+LEGS = {11: (3, 3), 9: (3, 2), 10: (-3, -2), 7: (2, 2), 8: (-2, -2)}
 DYS = [4, 3, -3, 2, -2, 1, -1, 0]
 DXS = [2, 1, -1, 0]
 WAYS = (1, -1)
-N_TAKE, POOL = 109, 2048
+N_TAKE, POOL = 114, 2048
 
 
 def part(span, way):
@@ -25,7 +26,7 @@
 
 def kernel(
     tok_in, gain_in, ids_in, wts_in, wg, wu, wd, out,
-    tok, gain, ids, wts, x_buf, normed, z_near, z_far, near_out, wgu, wdn, acc, y_buf, comb_hi, comb_lo,
+    tok, gain, ids, wts, x_buf, normed, z_near, z_far, mid_far, mid_last, near_out, wgu, wdn, acc, y_buf, comb_hi, comb_lo,
     ra_y, sa_y, za, ra_x, rb_x, sb_x, zb, rb_y, res, back,
     pool, w_sem, s_sem, r_sem,
 ):
@@ -55,16 +56,14 @@
     def greet(e, t):
         pl.semaphore_signal(barrier, inc=1, device_id=(e, t), device_id_type=MESH)
 
-    for off in OFF[::-1]:
+    for off in OFF[6:0:-1]:
         for c in range(2):
-            greet(2 * zm(off) + c, twin)
-            if off != 0:
-                greet(2 * zm(off) + c, tp)
+            greet(2 * zm(off) + c, tp)
     greet(2 * z + 1 - core, tp)
     for d in DYS[:-1]:
         greet(ep, tp_y(d))
-    greet(ep, tp_x(2))
-    greet(ep, tp_x(2 * half - 1))
+    for d in DXS[:-1]:
+        greet(ep, tp_x(d))
 
     loads = [
         pltpu.make_async_copy(tok_in, tok, w_sem.at[0]),
@@ -125,17 +124,8 @@
             device_id_type=MESH,
         ).wait_send()
 
-    for load in loads[:4]:
-        load.wait()
-
-    def norm_rows(i, carry):
-        rows = pl.ds(pl.multiple_of(i * 16, 16), 16)
-        values = tok[rows, :].astype(F32)
-        mean = jnp.mean(values * values, axis=-1, keepdims=True)
-        normed[rows, :] = (values * lax.rsqrt(mean + 1e-06) * gain[...]).astype(BF)
-        return carry
-
-    lax.fori_loop(0, 8, norm_rows, 0)
+    loads[2].wait()
+    loads[3].wait()
 
     lanes = lax.broadcasted_iota(jnp.int32, (128, 128), 1)
     rows = lax.broadcasted_iota(jnp.int32, (128, 128), 0)
@@ -155,6 +145,18 @@
     at = [(p == row) for p in pos]
     pick = (at[0] | at[1]).astype(F32).astype(BF)
 
+    loads[0].wait()
+    loads[1].wait()
+
+    def norm_rows(i, carry):
+        rows = pl.ds(pl.multiple_of(i * 16, 16), 16)
+        values = tok[rows, :].astype(F32)
+        mean = jnp.mean(values * values, axis=-1, keepdims=True)
+        normed[rows, :] = (values * lax.rsqrt(mean + 1e-06) * gain[...]).astype(BF)
+        return carry
+
+    lax.fori_loop(0, 8, norm_rows, 0)
+
     pair = lax.div(x, 2)
     column = pl.ds(pl.multiple_of(y * 256, 256), 256)
     rows_out = jnp.dot(pick[32:192], normed[:, column], preferred_element_type=F32)
@@ -165,19 +167,26 @@
         rows_out = jnp.dot(pick[192:], normed[:, column], preferred_element_type=F32)
         z_far[:, :, yy] = rows_out.astype(BF).reshape(6, 2, 16, 128)
 
-    pl.semaphore_wait(barrier, 24 + 22 + 1 + 7 + 2)
+    pl.semaphore_wait(barrier, 12 + 1 + 7 + 3)
 
     for p in range(1, 6):
         for c in range(2):
             send(("zn", (p - 1) // 2), z_near.at[p - 1, c], x_buf.at[y, :, core, p],
                  2 * zm(-OFF[p]) + c, tp)
-    for p in (11, 10, 9, 8, 7, 6):
+    def landing(p):
+        return x_buf.at[y, pair, half, p] if p >= LAST[0] else x_buf.at[:, pair, half, p]
+
+    def middle(p):
+        return mid_last.at[p - 9] if p >= LAST[0] else mid_far.at[p - 7]
+
+    for p in (*LEGS, 6):
         for c in range(2):
-            src, dst = z_far.at[p - 6, c], x_buf.at[:, pair, half, p]
-            if p >= LAST[0]:
-                src, dst = z_far.at[p - 6, c, y], x_buf.at[y, pair, half, p]
-            key = ("zl",) if p >= LAST[0] else ("zf",)
-            sent_z.append((message(key, src, dst, 2 * zm(-OFF[p]) + c, tp, 1), count(src)))
+            src = z_far.at[p - 6, c, y] if p >= LAST[0] else z_far.at[p - 6, c]
+            if p in LEGS:
+                copy = message(("mid", p), src, middle(p), 2 * zm(-LEGS[p][0]) + c, tp, 1)
+            else:
+                copy = message(("zf",), src, landing(p), 2 * zm(-OFF[p]) + c, tp, 1)
+            sent_z.append((copy, count(src)))
 
     @pl.when(core == half)
     def _():
@@ -203,6 +212,12 @@
     high = comb.astype(BF)
     comb_hi[...] = high
     comb_lo[...] = (comb - high.astype(F32)).astype(BF)
+
+    def hand_on(*tiles_held):
+        for p in tiles_held:
+            take(("mid", p), middle(p))
+            key = ("zl",) if p >= LAST[0] else ("zf",)
+            send(key, middle(p), landing(p), 2 * zm(-LEGS[p][1]) + core, tp)
 
     def gather_y(chunk, step):
         ps = pl.ds(*NEAR[chunk])
@@ -373,64 +388,75 @@
             total = total + rb_y[i].astype(F32)
         res[pl.ds(RB[0], RB[1])] = total.astype(BF)
 
-    for chunk in range(3):
-        gather_y(chunk, 1)
+    gather_y(0, 1)
+    gather_y(1, 1)
+    hand_on(*LEGS)
+    gather_y(2, 1)
+    gather_y(0, 2)
+    gather_y(1, 2)
     last_y()
     last_x(1, 0)
-    gather_y(0, 2)
+    gather_y(2, 2)
     gather_x(1)
-    gather_y(1, 2)
-    gather_y(2, 2)
     gather_y(0, 3)
+    gather_y(1, 3)
     last_x(1, 1, -1)
-    gather_y(1, 3)
     gather_y(2, 3)
-    last_x(1, 2, -2)
     gather_x(2)
     gather_y(0, 4)
-    last_x(1, 3, -3, 4)
-    last_x(2, 0, 1, -1)
+    last_x(1, 2, -2)
     gather_y(1, 4)
     gather_y(2, 4)
+    last_x(1, 3, -3, 4)
     take(("near",), x_buf.at[:, :, 1 - core, 0])
     loads[4].wait()
     loads[5].wait()
     for dy in (0, 1, -1):
         up(ym(dy), 0, dy == 0)
+    last_x(2, 0, 1, -1)
+    for dy in (2, -2):
+        up(ym(dy), 0, False)
     last_x(2, 2, -2)
-    for dy in (2, -2, 3, -3):
+    for dy in (3, -3):
         up(ym(dy), 0, False)
-    last_x(2, 3, -3, 4)
     for chunk in range(3):
         gather_y(chunk, 5)
     up(ym(4), 0, False)
     hidden = act()
     loads[6].wait()
-    for dy in DYS:
+    down(hidden, 4, 0)
+    ray(1)
+    for dy in DYS[1:4]:
         down(hidden, dy, 0)
-        if dy == 4:
-            ray(1)
+    last_x(2, 3, -3, 4)
+    for dy in DYS[4:]:
+        down(hidden, dy, 0)
     gather_x(3)
+    ray(2)
     last_x(3)
-    ray(2)
     for yy in range(NY):
         up(yy, 6, yy == 0)
     hidden = act()
-    for dy in DYS:
+    for dy in DYS[:4]:
         down(hidden, dy, 6)
         rbx(1, dy)
     ray(3)
-    for dy in DYS:
+    for dy in DYS[4:]:
+        down(hidden, dy, 6)
+        rbx(1, dy)
+    for dy in DYS[:3]:
+        rbx(2, dy)
+    ray(4)
+    for dy in DYS[3:]:
         rbx(2, dy)
     for dy in DYS[:3]:
         rbx(3, dy)
-    ray(4)
+    for dx in DXS[:3]:
+        ray_end(dx)
+        rax(dx)
     for dy in DYS[3:]:
         rbx(3, dy)
-    for dx in DXS:
-        ray_end(dx)
-        if dx:
-            rax(dx)
+    ray_end(0)
 
     def give(span):
         for p in range(span[0] + span[1] - 1, span[0] - 1, -1):
@@ -459,8 +485,8 @@
     rows_in = back[...].reshape(384, 128)
     mixed = jnp.dot(comb_hi[...], rows_in, preferred_element_type=F32)
     mixed = mixed + jnp.dot(comb_lo[...], rows_in, preferred_element_type=F32)
-    mixed = jnp.where(half == 1, pltpu.roll(mixed, 64, 1), mixed)
-    out[...] = mixed[:, :64].astype(BF)
+    mixed = jnp.transpose(mixed)
+    out[...] = jnp.where(half == 1, mixed[64:], mixed[:64]).astype(BF)
 
     wait_sent(0, sum(sent))
 
@@ -481,7 +507,7 @@
     a, b = RA[1], RB[1]
     return pl.pallas_call(
         kernel,
-        out_shape=jax.ShapeDtypeStruct((128, 64), BF),
+        out_shape=jax.ShapeDtypeStruct((64, 128), BF),
         in_specs=[hbm] * 7,
         out_specs=vmem,
         scratch_shapes=[
@@ -493,6 +519,8 @@
             pltpu.VMEM((128, 2048), BF),
             tiles(5, 2, 2),
             tiles(6, 2, NY),
+            tiles(2, NY),
+            tiles(3),
             tiles(NY, 2),
             pltpu.VMEM((2048, 768), BF),
             pltpu.VMEM((384, 2048), BF),
@@ -516,7 +544,7 @@
     )(
         tokens, norm_gain.reshape(1, -1), route_ids.T, route_weights.T,
         gate_proj, up_proj, down_proj,
-    )
+    ).T
 
 
 def solution(mesh):

time: 70.8 us -> 68.3 us (0.965)
  Pallas kernels: 69.1 us -> 66.8 us
    pallas_call x1, Pallas kernels: 69.1 us -> 66.8 us  [per_device(): pl.pallas_call(kernel, out_shape=jax.ShapeDtypeStruct((64, 128), BF), in_...]
    pallas_call x1 -> x0, local copies, waits for them, and re-layouts: 1.45 us -> none  [per_device(): pl.pallas_call(kernel, out_shape=jax.ShapeDtypeStruct((128, 64), BF), in_...]
    unnamed x0 -> x1, local copies, waits for them, and re-layouts: none -> 1.32 us
where the time goes in v3:
time: 68.3 us; the launch traced here: 68.1 us
  Pallas kernels  66.8 us (98%)
  local copies, waits for them, and re-layouts  1.32 us (2%)
    pallas_call x1, Pallas kernels, per_device(): pl.pallas_call(kernel, out_shape=jax.ShapeDtypeStruct((64, 128), BF), in_...  66.8 us

profile of v3, /device:TPU:1, one launch (start us, length us, event | category | flops | bytes accessed | tf_op | source)
XLA Modules:
  0.0 68.1 jit_solution(5778377004643084832)
XLA Ops:
  0.0 66.8 %shard_map.73 = bf16[64,128]{1,0:T(8,128)(2,1)} custom-call(bf16[128,2048]{1,0:T(8,128)(2,1)} %tok_in.1, f32[1,2048]{1,0:T(1,128)} %bitcast.5, s32[2,128]{1,0:T(2,128)} %bitcast.6, f32[2,128]{1,0:T(2,128)} %bitcast.7, bf16[1,2048,384]{2,1,0:T(8,128)(2,1)} %wg.1, bf16[1,2048,384]{2,1,0:T(8,128)(2,1)} %wu.1, bf16[1,384,2048]{2,1,0:T(8,128)(2,1)} %wd.1), custom_call_target="tpu_custom_call" | custom-call | flops 2000000000 | bytes 6000000 | tf_op jit(solution)/shard_map/pallas_call | solution.py:508
  66.8 1.3 %copy.9 = bf16[128,64]{0,1:T(8,128)(2,1)} copy(bf16[128,64]{0,1:T(8,128)(2,1)} %bitcast.4) | data formatting | bytes 32768

commit v4 on v3

--- a/solution.py
+++ b/solution.py
@@ -60,7 +60,7 @@
         for c in range(2):
             greet(2 * zm(off) + c, tp)
     greet(2 * z + 1 - core, tp)
-    for d in DYS[:-1]:
+    for d in DYS[3:-1]:
         greet(ep, tp_y(d))
     for d in DXS[:-1]:
         greet(ep, tp_x(d))
@@ -167,7 +167,7 @@
         rows_out = jnp.dot(pick[192:], normed[:, column], preferred_element_type=F32)
         z_far[:, :, yy] = rows_out.astype(BF).reshape(6, 2, 16, 128)
 
-    pl.semaphore_wait(barrier, 12 + 1 + 7 + 3)
+    pl.semaphore_wait(barrier, 12 + 1 + 4 + 3)
 
     for p in range(1, 6):
         for c in range(2):
@@ -256,10 +256,11 @@
             src = column_of(rows, xx, ps)
             send(("gx", step, w) if step == 1 else ("gx", 2), src, src, ep, tp_x(w))
 
-    def last_y():
+    def last_y(dys):
         src = x_buf.at[y, pair, half, pl.ds(*LAST)]
-        take(("zl",), src)
-        for dy in DYS[:7]:
+        if len(dys) > 1:
+            take(("zl",), src)
+        for dy in dys:
             send(("ly", dy), src, src, ep, tp_y(dy))
 
     def last_x(step, *dys):
@@ -394,11 +395,12 @@
     gather_y(2, 1)
     gather_y(0, 2)
     gather_y(1, 2)
-    last_y()
+    last_y(DYS[1:7])
     last_x(1, 0)
     gather_y(2, 2)
     gather_x(1)
     gather_y(0, 3)
+    last_y(DYS[:1])
     gather_y(1, 3)
     last_x(1, 1, -1)
     gather_y(2, 3)
@@ -444,19 +446,17 @@
     for dy in DYS[4:]:
         down(hidden, dy, 6)
         rbx(1, dy)
-    for dy in DYS[:3]:
+    for dy in DYS:
         rbx(2, dy)
     ray(4)
-    for dy in DYS[3:]:
-        rbx(2, dy)
     for dy in DYS[:3]:
         rbx(3, dy)
-    for dx in DXS[:3]:
+    for dx, dys in zip(DXS, ((2, -2), (1, -1), (0,), ())):
+        for dy in dys:
+            rbx(3, dy)
         ray_end(dx)
-        rax(dx)
-    for dy in DYS[3:]:
-        rbx(3, dy)
-    ray_end(0)
+        if dx:
+            rax(dx)
 
     def give(span):
         for p in range(span[0] + span[1] - 1, span[0] - 1, -1):
@@ -465,10 +465,10 @@
             if p > 0:
                 send(("back",), res.at[p], back.at[p, core], e, tp)
 
+    rby_end()
+    give(RB)
     rax_end()
     give(RA)
-    rby_end()
-    give(RB)
     near_back = message(("back",), res.at[0], back.at[0, core], 2 * z + half, tp, 2)
 
     @pl.when(half == core)

time: 68.3 us -> 67.1 us (0.982)
  Pallas kernels: 66.8 us -> 65.6 us
    pallas_call x1, Pallas kernels: 66.8 us -> 65.6 us  [per_device(): pl.pallas_call(kernel, out_shape=jax.ShapeDtypeStruct((64, 128), BF), in_...]
where the time goes in v4:
time: 67.1 us; the launch traced here: 66.9 us
  Pallas kernels  65.6 us (98%)
  local copies, waits for them, and re-layouts  1.32 us (2%)
    pallas_call x1, Pallas kernels, per_device(): pl.pallas_call(kernel, out_shape=jax.ShapeDtypeStruct((64, 128), BF), in_...  65.6 us

profile of v4, /device:TPU:1, one launch (start us, length us, event | category | flops | bytes accessed | tf_op | source)
XLA Modules:
  0.0 66.9 jit_solution(13070042777378427404)
XLA Ops:
  0.0 65.6 %shard_map.73 = bf16[64,128]{1,0:T(8,128)(2,1)} custom-call(bf16[128,2048]{1,0:T(8,128)(2,1)} %tok_in.1, f32[1,2048]{1,0:T(1,128)} %bitcast.5, s32[2,128]{1,0:T(2,128)} %bitcast.6, f32[2,128]{1,0:T(2,128)} %bitcast.7, bf16[1,2048,384]{2,1,0:T(8,128)(2,1)} %wg.1, bf16[1,2048,384]{2,1,0:T(8,128)(2,1)} %wu.1, bf16[1,384,2048]{2,1,0:T(8,128)(2,1)} %wd.1), custom_call_target="tpu_custom_call" | custom-call | flops 2000000000 | bytes 6000000 | tf_op jit(solution)/shard_map/pallas_call | solution.py:508
  65.6 1.3 %copy.9 = bf16[128,64]{0,1:T(8,128)(2,1)} copy(bf16[128,64]{0,1:T(8,128)(2,1)} %bitcast.4) | data formatting | bytes 32768
